TPU v7x, 32 devices: a whole 2x2x4 slice. The times are simulated.
32 devices in a mesh: sp: 16 (over z, y, x), tp: 2 (over core).
Axes of the slice: x: 2, y: 2, z: 4, core: 2. Of those that a mesh axis runs over, the one named last changes fastest.
Arguments:
- stream_in: bfloat16 [4096, 2048], P('sp'), may hold values from -6 to 6
- norm_gain: float32 [2, 2048], replicated, may hold values from 0.1 to 1.9
- value_weight: bfloat16 [2, 2048, 2048], P(None, 'sp', 'tp'), may hold values from -0.125 to 0.125
- gate_weight: bfloat16 [2, 2048, 2048], P(None, 'sp', 'tp'), may hold values from -0.125 to 0.125
- conv_taps: float32 [2, 31, 2048], P(None, None, 'tp'), may hold values from -5 to 5
- channel_gain: float32 [2, 2048], P(None, 'tp'), may hold values from 0.1 to 1.9
- out_weight: bfloat16 [2, 2048, 2048], P(None, 'tp', 'sp'), may hold values from -0.125 to 0.125
Outputs:
- stream_out: bfloat16 [4096, 2048], P('sp')
All inputs are finite; a program needn't handle non-finite values.
Results may differ from a plain program's by a relative error of at most 0.015.
Values may be sent and summed in bfloat16 or wider, within the bound.
A program may use at most 64 MiB of HBM per device.

v0:
```python
import jax
import jax.numpy as jnp
from jax import lax
from jax.sharding import PartitionSpec as P

LAYERS = 2
epsilon = 1e-05


def passed_along(value, axis, steps):
    count = lax.axis_size(axis)
    leading, last = (max(0, -steps), min(count, count - steps))
    return lax.ppermute(value, axis, [(source, source + steps) for source in range(leading, last)])


def body(stream_in, norm_gain, value_weight, gate_weight, conv_taps, channel_gain, out_weight):
    stream = stream_in
    tok_rows = stream_in.shape[0]
    width = stream_in.shape[1]
    kernel = conv_taps.shape[1]
    local_cols = value_weight.shape[2]
    for layer in range(LAYERS):
        wide = stream.astype(jnp.float32)
        normed = (
            wide
            * lax.rsqrt(jnp.mean(wide * wide, axis=1, keepdims=True) + epsilon)
            * norm_gain[layer]
        ).astype(jnp.bfloat16)
        value = jnp.dot(
            normed,
            lax.all_gather(value_weight[layer], "sp", axis=0, tiled=True),
            preferred_element_type=jnp.float32,
        )
        gate = jnp.dot(
            normed,
            lax.all_gather(gate_weight[layer], "sp", axis=0, tiled=True),
            preferred_element_type=jnp.float32,
        )
        gated = (value * jax.nn.sigmoid(gate)).astype(jnp.bfloat16)
        earlier = passed_along(gated[tok_rows - (kernel - 1) :], "sp", 1)
        padded = jnp.concatenate([earlier, gated], axis=0).astype(jnp.float32)
        taps = conv_taps[layer]
        filtered = jnp.zeros((tok_rows, local_cols), jnp.float32)
        for tap in range(kernel):
            filtered = filtered + taps[tap] * padded[tap : tap + tok_rows]
        sum_first, sum_second = lax.psum(
            (jnp.sum(filtered, axis=1), jnp.sum(filtered * filtered, axis=1)), "tp"
        )
        mean_value = (sum_first / width)[:, None]
        variance = (sum_second / width)[:, None] - mean_value * mean_value
        activated = jax.nn.silu(
            (filtered - mean_value) * lax.rsqrt(variance + epsilon) * channel_gain[layer]
        ).astype(jnp.bfloat16)
        whole_out = lax.all_gather(out_weight[layer], "sp", axis=1, tiled=True)
        terms = jnp.dot(activated, whole_out, preferred_element_type=jnp.float32)
        summed = lax.psum(terms.astype(jnp.bfloat16), "tp").astype(jnp.float32)
        stream = (wide + summed).astype(jnp.bfloat16)
    return stream


def solution(mesh):
    return jax.shard_map(
        body,
        mesh=mesh,
        in_specs=(
            P("sp", None),
            P(),
            P(None, "sp", "tp"),
            P(None, "sp", "tp"),
            P(None, None, "tp"),
            P(None, "tp"),
            P(None, "tp", "sp"),
        ),
        out_specs=P("sp", None),
        check_vma=False,
    )
```

profile of v0, /device:TPU:0, one launch (start us, length us, event | category | flops | bytes accessed | tf_op | source)
XLA Modules:
  0.0 556.1 jit_solution(6253315192449355150)
XLA Ops:
  6.5 2.0 fusion.142
  8.5 0.0 all-gather.15.cloned.1.call-update
  8.6 0.0 all-gather.13.cloned.1.call-start
  8.6 1.9 fusion.141
  10.5 0.0 all-gather.13.cloned.1.call-update
  10.6 0.0 all-gather.17.cloned.1.call-start
  10.6 0.8 fusion.143
  11.4 0.0 all-gather.17.cloned.1.call-update
  11.5 0.0 all-reduce.5.cloned.1.call-start
  11.5 0.3 fusion.18
  11.9 0.1 fusion.146
  11.9 0.1 fusion.145
  12.0 76.4 %all-gather.15.cloned.1.call-done = bf16[1,2048,1024]{2,1,0:T(8,128)(2,1)} async-done(((bf16[1,128,1024]{2,1,0:T(8,128)(2,1)}), bf16[1,2048,1024]{2,1,0:T(8,128)(2,1)}) %all-gather.15.cloned.1.call-update) | async-done | bytes 4194320 | tf_op jit(solution)/shard_map/all_gather | solution.py:36
  88.5 3.6 fusion.56
  92.1 73.4 %all-gather.13.cloned.1.call-done = bf16[1,2048,1024]{2,1,0:T(8,128)(2,1)} async-done(((bf16[1,128,1024]{2,1,0:T(8,128)(2,1)}), bf16[1,2048,1024]{2,1,0:T(8,128)(2,1)}) %all-gather.13.cloned.1.call-update) | async-done | bytes 4194320 | tf_op jit(solution)/shard_map/all_gather | solution.py:31
  165.4 3.5 fusion.53
  169.0 3.4 collective-permute-start
  172.4 1.9 collective-permute-done
  174.2 0.2 maximum_convert_fusion
  174.4 5.8 %fusion.137 = (f32[256]{0:T(256)S(1)}, f32[256]{0:T(256)S(1)}, f32[256,1024]{1,0:T(8,128)S(1)}) fusion(f32[286,1024]{1,0:T(8,128)S(1)} %maximum_convert_fusion, f32[1024]{0:T(1024)S(1)} %bitcast.146, f32[1024]{0:T(1024)S(1)} %bitcast.147, f32[1024]{0:T(1024)S(1)} %bitcast.148, f32[1024]{0:T(1024)S(1)} %bitcast.149, f32[1024]{0:T(1024)S(1)} %bitcast.150, ...), kind=kLoop, calls=%fused_computation.185 | loop fusion | flops 16776704 | bytes 33683456 | tf_op jit(solution)/shard_map/reduce_sum | solution.py:47
  180.2 2.5 all-reduce.1
  182.7 72.8 %all-gather.17.cloned.1.call-done = bf16[1,1024,2048]{2,1,0:T(8,128)(2,1)} async-done(((bf16[1,1024,128]{2,1,0:T(8,128)(2,1)}), bf16[1,1024,2048]{2,1,0:T(8,128)(2,1)}) %all-gather.17.cloned.1.call-update) | async-done | bytes 4194320 | tf_op jit(solution)/shard_map/all_gather | solution.py:54
  255.5 4.7 fusion.12
  260.2 0.0 all-reduce.5.cloned.1.call-update
  260.2 0.0 all-gather.21.cloned.1.call-start
  260.3 0.5 all-gather.21.cloned.1.call-update
  260.8 0.0 all-gather.19.cloned.1.call-start
  260.9 0.5 all-gather.19.cloned.1.call-update
  261.4 0.0 all-gather.23.cloned.1.call-start
  261.4 0.7 all-gather.23.cloned.1.call-update
  262.1 0.0 all-reduce.7.cloned.1.call-start
  262.2 15.8 %all-reduce.5.cloned.1.call-done = bf16[256,2048]{1,0:T(8,128)(2,1)} async-done(((bf16[256,2048]{1,0:T(8,128)(2,1)}), bf16[256,2048]{1,0:T(8,128)(2,1)}) %all-reduce.5.cloned.1.call-update) | async-done | bytes 1048592 | tf_op jit(solution)/shard_map/psum | solution.py:56
  278.0 1.7 fusion.22
  279.7 77.7 %all-gather.21.cloned.1.call-done = bf16[1,2048,1024]{2,1,0:T(8,128)(2,1)} async-done(((bf16[1,128,1024]{2,1,0:T(8,128)(2,1)}), bf16[1,2048,1024]{2,1,0:T(8,128)(2,1)}) %all-gather.21.cloned.1.call-update) | async-done | bytes 4194320 | tf_op jit(solution)/shard_map/all_gather | solution.py:36
  357.4 3.6 fusion.59
  361.0 73.3 %all-gather.19.cloned.1.call-done = bf16[1,2048,1024]{2,1,0:T(8,128)(2,1)} async-done(((bf16[1,128,1024]{2,1,0:T(8,128)(2,1)}), bf16[1,2048,1024]{2,1,0:T(8,128)(2,1)}) %all-gather.19.cloned.1.call-update) | async-done | bytes 4194320 | tf_op jit(solution)/shard_map/all_gather | solution.py:31
  434.3 3.5 fusion.50
  437.8 3.5 collective-permute-start.1
  441.4 0.1 fusion.144
  441.5 1.6 collective-permute-done.1
  443.1 0.1 maximum_convert_fusion.1
  443.2 5.8 %fusion.136 = (f32[256]{0:T(256)S(1)}, f32[256]{0:T(256)S(1)}, f32[256,1024]{1,0:T(8,128)S(1)}) fusion(f32[286,1024]{1,0:T(8,128)S(1)} %maximum_convert_fusion.1, f32[1024]{0:T(1024)S(1)} %bitcast.112, f32[1024]{0:T(1024)S(1)} %bitcast.113, f32[1024]{0:T(1024)S(1)} %bitcast.156, f32[1024]{0:T(1024)S(1)} %bitcast.157, f32[1024]{0:T(1024)S(1)} %bitcast.158, ...), kind=kLoop, calls=%fused_computation.184 | loop fusion | flops 16776704 | bytes 33683456 | tf_op jit(solution)/shard_map/reduce_sum | solution.py:47
  449.1 2.5 all-reduce
  451.5 72.8 %all-gather.23.cloned.1.call-done = bf16[1,1024,2048]{2,1,0:T(8,128)(2,1)} async-done(((bf16[1,1024,128]{2,1,0:T(8,128)(2,1)}), bf16[1,1024,2048]{2,1,0:T(8,128)(2,1)}) %all-gather.23.cloned.1.call-update) | async-done | bytes 4194320 | tf_op jit(solution)/shard_map/all_gather | solution.py:54
  524.3 4.7 fusion.15
  529.0 0.0 all-reduce.7.cloned.1.call-update
  529.0 17.8 %all-reduce.7.cloned.1.call-done = bf16[256,2048]{1,0:T(8,128)(2,1)} async-done(((bf16[256,2048]{1,0:T(8,128)(2,1)}), bf16[256,2048]{1,0:T(8,128)(2,1)}) %all-reduce.7.cloned.1.call-update) | async-done | bytes 1048592 | tf_op jit(solution)/shard_map/psum | solution.py:56
  546.8 2.5 fusion.25
  (20 shorter events, 0.1 us)
Async XLA Ops:
  6.5 4.1 copy-start.1
  6.5 5.0 copy-start
  6.5 81.9 %all-gather.15.cloned.1.call-start = ((), (), s32[]{:S(2)}) async-start(), calls=%async_computation.3 | async-start | bytes 4456448 | tf_op jit(solution)/shard_map/all_gather | solution.py:36
  8.5 3.3 copy-start.2
  8.5 3.5 copy-start.3
  8.6 156.9 %all-gather.13.cloned.1.call-start = ((), (), s32[]{:S(2)}) async-start(), calls=%async_computation.2 | async-start | bytes 4456448 | tf_op jit(solution)/shard_map/all_gather | solution.py:31
  10.6 244.9 %all-gather.17.cloned.1.call-start = ((), (), s32[]{:S(2)}) async-start(), calls=%async_computation.4 | async-start | bytes 4456448 | tf_op jit(solution)/shard_map/all_gather | solution.py:54
  11.5 266.5 %all-reduce.5.cloned.1.call-start = ((), (), s32[]{:S(2)}) async-start(), calls=%async_computation | async-start | bytes 2097152 | tf_op jit(solution)/shard_map/psum | solution.py:56
  92.0 80.3 %copy-start.4 = (f32[2,1024]{1,0:T(2,128)S(1)}, f32[2,1024]{1,0:T(2,128)}, u32[]{:S(2)}) copy-start(f32[2,1024]{1,0:T(2,128)} %param.12) | copy-start | bytes 24580
  169.0 5.2 collective-permute-start
  260.2 97.2 %all-gather.21.cloned.1.call-start = ((), (), s32[]{:S(2)}) async-start(), calls=%async_computation.6 | async-start | bytes 4456448 | tf_op jit(solution)/shard_map/all_gather | solution.py:36
  260.8 173.5 %all-gather.19.cloned.1.call-start = ((), (), s32[]{:S(2)}) async-start(), calls=%async_computation.5 | async-start | bytes 4456448 | tf_op jit(solution)/shard_map/all_gather | solution.py:31
  261.4 262.9 %all-gather.23.cloned.1.call-start = ((), (), s32[]{:S(2)}) async-start(), calls=%async_computation.7 | async-start | bytes 4456448 | tf_op jit(solution)/shard_map/all_gather | solution.py:54
  262.1 284.6 %all-reduce.7.cloned.1.call-start = ((), (), s32[]{:S(2)}) async-start(), calls=%async_computation.1 | async-start | bytes 2097152 | tf_op jit(solution)/shard_map/psum | solution.py:56
  437.8 5.3 collective-permute-start.1
Sparse Core Ops, SparseCore 0:
  10.1 78.3 all-gather.14
  91.2 74.1 all-gather.12
  168.2 87.3 all-gather.16
  260.3 17.5 all-reduce.4
  280.6 76.7 all-gather.20
  360.0 74.1 all-gather.18
  437.0 87.3 all-gather.22
  529.1 17.5 all-reduce.6
where the time goes:
time: 557 us; the launch traced here: 556 us
  waiting for transfers between devices  485 us (87%)
  matrix products  23.6 us (4%)
  other arithmetic  16.5 us (3%)
  between operations  13.7 us (2%)
  starting transfers between devices  7.18 us (1%)
    all_gather x2, waiting for transfers between devices, body(): lax.all_gather(gate_weight[layer], 'sp', axis=0, tiled=True)  154 us
    all_gather x2, waiting for transfers between devices, body(): lax.all_gather(value_weight[layer], 'sp', axis=0, tiled=True)  147 us
    all_gather x2, waiting for transfers between devices, body(): whole_out = lax.all_gather(out_weight[layer], 'sp', axis=1, tiled=True)  146 us
    psum x2, waiting for transfers between devices, body(): summed = lax.psum(terms.astype(jnp.bfloat16), 'tp').astype(jnp.float32)  33.6 us
    reduce_sum x2, other arithmetic, body(): jnp.sum(filtered, axis=1)  11.6 us
  transfers between devices with their start and end apart: 10, of which 10 were waited for; matrix products, arithmetic and copies ran while one was open for 6% of the time, Pallas kernels for 0%

commit v1 on v0

--- a/solution.py
+++ b/solution.py
@@ -5,6 +5,12 @@
 
 LAYERS = 2
 epsilon = 1e-05
+
+
+def gather_and_add(x, name):
+    parts = lax.all_gather(x, name, axis=0, tiled=False)
+    total = parts.sum(axis=0)
+    return total
 
 
 def passed_along(value, axis, steps):
@@ -53,7 +59,7 @@
         ).astype(jnp.bfloat16)
         whole_out = lax.all_gather(out_weight[layer], "sp", axis=1, tiled=True)
         terms = jnp.dot(activated, whole_out, preferred_element_type=jnp.float32)
-        summed = lax.psum(terms.astype(jnp.bfloat16), "tp").astype(jnp.float32)
+        summed = gather_and_add(terms.astype(jnp.bfloat16), "tp").astype(jnp.float32)
         stream = (wide + summed).astype(jnp.bfloat16)
     return stream
 

time: 557 us -> 540 us (0.969)
  waiting for transfers between devices: 485 us -> 467 us
    psum x2 -> x0, waiting for transfers between devices: 33.6 us -> none  [body(): summed = lax.psum(terms.astype(jnp.bfloat16), 'tp').astype(jnp.float32)]
    all_gather x0 -> x2, waiting for transfers between devices: none -> 15.9 us  [gather_and_add(): parts = lax.all_gather(x, name, axis=0, tiled=False)]
where the time goes in v1:
time: 540 us; the launch traced here: 539 us
  waiting for transfers between devices  467 us (86%)
  matrix products  23.6 us (4%)
  other arithmetic  18.4 us (3%)
  between operations  13.7 us (3%)
  starting transfers between devices  7.17 us (1%)
    all_gather x2, waiting for transfers between devices, body(): lax.all_gather(gate_weight[layer], 'sp', axis=0, tiled=True)  153 us
    all_gather x2, waiting for transfers between devices, body(): lax.all_gather(value_weight[layer], 'sp', axis=0, tiled=True)  147 us
    all_gather x2, waiting for transfers between devices, body(): whole_out = lax.all_gather(out_weight[layer], 'sp', axis=1, tiled=True)  146 us
    all_gather x2, waiting for transfers between devices, gather_and_add(): parts = lax.all_gather(x, name, axis=0, tiled=False)  15.9 us
    reduce_sum x2, other arithmetic, body(): jnp.sum(filtered, axis=1)  11.6 us
  transfers between devices with their start and end apart: 10, of which 10 were waited for; matrix products, arithmetic and copies ran while one was open for 6% of the time, Pallas kernels for 0%

profile of v1, /device:TPU:0, one launch (start us, length us, event | category | flops | bytes accessed | tf_op | source)
XLA Modules:
  0.0 539.4 jit_solution(2713619507272308410)
XLA Ops:
  6.5 2.0 fusion.142
  8.6 0.0 all-gather.19.cloned.1.call-update
  8.6 0.0 all-gather.17.cloned.1.call-start
  8.7 1.9 fusion.141
  10.6 0.0 all-gather.17.cloned.1.call-update
  10.6 0.0 all-gather.21.cloned.1.call-start
  10.7 0.8 fusion.143
  11.5 0.0 all-gather.21.cloned.1.call-update
  11.5 0.0 all-gather.23.cloned.1.call-start
  11.6 0.3 fusion.18
  11.9 0.1 fusion.146
  12.0 0.1 fusion.145
  12.1 76.3 %all-gather.19.cloned.1.call-done = bf16[1,2048,1024]{2,1,0:T(8,128)(2,1)} async-done(((bf16[1,128,1024]{2,1,0:T(8,128)(2,1)}), bf16[1,2048,1024]{2,1,0:T(8,128)(2,1)}) %all-gather.19.cloned.1.call-update) | async-done | bytes 4194320 | tf_op jit(solution)/shard_map/all_gather | solution.py:42
  88.5 3.6 fusion.56
  92.1 73.4 %all-gather.17.cloned.1.call-done = bf16[1,2048,1024]{2,1,0:T(8,128)(2,1)} async-done(((bf16[1,128,1024]{2,1,0:T(8,128)(2,1)}), bf16[1,2048,1024]{2,1,0:T(8,128)(2,1)}) %all-gather.17.cloned.1.call-update) | async-done | bytes 4194320 | tf_op jit(solution)/shard_map/all_gather | solution.py:37
  165.4 3.5 fusion.53
  169.0 3.4 collective-permute-start
  172.4 1.9 collective-permute-done
  174.2 0.2 maximum_convert_fusion
  174.4 5.8 %fusion.137 = (f32[256]{0:T(256)S(1)}, f32[256]{0:T(256)S(1)}, f32[256,1024]{1,0:T(8,128)S(1)}) fusion(f32[286,1024]{1,0:T(8,128)S(1)} %maximum_convert_fusion, f32[1024]{0:T(1024)S(1)} %bitcast.150, f32[1024]{0:T(1024)S(1)} %bitcast.151, f32[1024]{0:T(1024)S(1)} %bitcast.152, f32[1024]{0:T(1024)S(1)} %bitcast.153, f32[1024]{0:T(1024)S(1)} %bitcast.154, ...), kind=kLoop, calls=%fused_computation.185 | loop fusion | flops 16776704 | bytes 33683456 | tf_op jit(solution)/shard_map/reduce_sum | solution.py:53
  180.2 2.5 all-reduce.1
  182.7 72.8 %all-gather.21.cloned.1.call-done = bf16[1,1024,2048]{2,1,0:T(8,128)(2,1)} async-done(((bf16[1,1024,128]{2,1,0:T(8,128)(2,1)}), bf16[1,1024,2048]{2,1,0:T(8,128)(2,1)}) %all-gather.21.cloned.1.call-update) | async-done | bytes 4194320 | tf_op jit(solution)/shard_map/all_gather | solution.py:60
  255.5 4.7 fusion.12
  260.2 0.0 all-gather.27.cloned.1.call-start
  260.3 0.5 all-gather.27.cloned.1.call-update
  260.8 0.0 all-gather.25.cloned.1.call-start
  260.9 0.5 all-gather.25.cloned.1.call-update
  261.4 0.0 all-gather.29.cloned.1.call-start
  261.4 0.7 all-gather.29.cloned.1.call-update
  262.1 0.0 all-gather.31.cloned.1.call-start
  262.2 6.9 %all-gather.23.cloned.1.call-done = bf16[512,2048]{1,0:T(8,128)(2,1)} async-done(((bf16[256,2048]{1,0:T(8,128)(2,1)}), bf16[512,2048]{1,0:T(8,128)(2,1)}) %all-gather.23.cloned.1.call-update) | async-done | bytes 2097168 | tf_op jit(solution)/shard_map/all_gather | solution.py:11
  269.1 2.1 reduce_sum.81
  271.3 0.5 fusion.22
  271.8 76.8 %all-gather.27.cloned.1.call-done = bf16[1,2048,1024]{2,1,0:T(8,128)(2,1)} async-done(((bf16[1,128,1024]{2,1,0:T(8,128)(2,1)}), bf16[1,2048,1024]{2,1,0:T(8,128)(2,1)}) %all-gather.27.cloned.1.call-update) | async-done | bytes 4194320 | tf_op jit(solution)/shard_map/all_gather | solution.py:42
  348.5 3.6 fusion.59
  352.1 73.3 %all-gather.25.cloned.1.call-done = bf16[1,2048,1024]{2,1,0:T(8,128)(2,1)} async-done(((bf16[1,128,1024]{2,1,0:T(8,128)(2,1)}), bf16[1,2048,1024]{2,1,0:T(8,128)(2,1)}) %all-gather.25.cloned.1.call-update) | async-done | bytes 4194320 | tf_op jit(solution)/shard_map/all_gather | solution.py:37
  425.4 3.5 fusion.50
  428.9 3.5 collective-permute-start.1
  432.5 0.1 fusion.144
  432.6 1.6 collective-permute-done.1
  434.2 0.1 maximum_convert_fusion.1
  434.3 5.8 %fusion.136 = (f32[256]{0:T(256)S(1)}, f32[256]{0:T(256)S(1)}, f32[256,1024]{1,0:T(8,128)S(1)}) fusion(f32[286,1024]{1,0:T(8,128)S(1)} %maximum_convert_fusion.1, f32[1024]{0:T(1024)S(1)} %bitcast.116, f32[1024]{0:T(1024)S(1)} %bitcast.117, f32[1024]{0:T(1024)S(1)} %bitcast.160, f32[1024]{0:T(1024)S(1)} %bitcast.161, f32[1024]{0:T(1024)S(1)} %bitcast.162, ...), kind=kLoop, calls=%fused_computation.184 | loop fusion | flops 16776704 | bytes 33683456 | tf_op jit(solution)/shard_map/reduce_sum | solution.py:53
  440.2 2.5 all-reduce
  442.7 72.8 %all-gather.29.cloned.1.call-done = bf16[1,1024,2048]{2,1,0:T(8,128)(2,1)} async-done(((bf16[1,1024,128]{2,1,0:T(8,128)(2,1)}), bf16[1,1024,2048]{2,1,0:T(8,128)(2,1)}) %all-gather.29.cloned.1.call-update) | async-done | bytes 4194320 | tf_op jit(solution)/shard_map/all_gather | solution.py:60
  515.4 4.7 fusion.15
  520.1 8.9 %all-gather.31.cloned.1.call-done = bf16[512,2048]{1,0:T(8,128)(2,1)} async-done(((bf16[256,2048]{1,0:T(8,128)(2,1)}), bf16[512,2048]{1,0:T(8,128)(2,1)}) %all-gather.31.cloned.1.call-update) | async-done | bytes 2097168 | tf_op jit(solution)/shard_map/all_gather | solution.py:11
  529.1 2.1 reduce_sum.85
  531.2 1.4 fusion.25
  (22 shorter events, 0.2 us)
Async XLA Ops:
  6.5 4.1 copy-start.1
  6.5 5.0 copy-start
  6.5 81.9 %all-gather.19.cloned.1.call-start = ((), (), s32[]{:S(2)}) async-start(), calls=%async_computation.1 | async-start | bytes 4456448 | tf_op jit(solution)/shard_map/all_gather | solution.py:42
  8.6 3.3 copy-start.2
  8.6 3.5 copy-start.3
  8.6 156.8 %all-gather.17.cloned.1.call-start = ((), (), s32[]{:S(2)}) async-start(), calls=%async_computation | async-start | bytes 4456448 | tf_op jit(solution)/shard_map/all_gather | solution.py:37
  10.6 244.9 %all-gather.21.cloned.1.call-start = ((), (), s32[]{:S(2)}) async-start(), calls=%async_computation.2 | async-start | bytes 4456448 | tf_op jit(solution)/shard_map/all_gather | solution.py:60
  11.5 257.6 %all-gather.23.cloned.1.call-start = ((), (), s32[]{:S(2)}) async-start(), calls=%async_computation.3 | async-start | bytes 3145728 | tf_op jit(solution)/shard_map/all_gather | solution.py:11
  92.0 80.3 %copy-start.4 = (f32[2,1024]{1,0:T(2,128)S(1)}, f32[2,1024]{1,0:T(2,128)}, u32[]{:S(2)}) copy-start(f32[2,1024]{1,0:T(2,128)} %param.12) | copy-start | bytes 24580
  169.0 5.2 collective-permute-start
  260.2 88.3 %all-gather.27.cloned.1.call-start = ((), (), s32[]{:S(2)}) async-start(), calls=%async_computation.5 | async-start | bytes 4456448 | tf_op jit(solution)/shard_map/all_gather | solution.py:42
  260.8 164.6 %all-gather.25.cloned.1.call-start = ((), (), s32[]{:S(2)}) async-start(), calls=%async_computation.4 | async-start | bytes 4456448 | tf_op jit(solution)/shard_map/all_gather | solution.py:37
  261.4 254.0 %all-gather.29.cloned.1.call-start = ((), (), s32[]{:S(2)}) async-start(), calls=%async_computation.6 | async-start | bytes 4456448 | tf_op jit(solution)/shard_map/all_gather | solution.py:60
  262.1 266.9 %all-gather.31.cloned.1.call-start = ((), (), s32[]{:S(2)}) async-start(), calls=%async_computation.7 | async-start | bytes 3145728 | tf_op jit(solution)/shard_map/all_gather | solution.py:11
  428.9 5.2 collective-permute-start.1
Sparse Core Ops, SparseCore 0:
  10.1 78.3 all-gather.18
  91.2 74.1 all-gather.16
  168.2 87.3 all-gather.20
  260.3 8.7 all-gather.22
  271.7 76.7 all-gather.26
  351.2 74.1 all-gather.24
  428.1 87.3 all-gather.28
  520.3 8.7 all-gather.30
